TPU v7x, 32 devices: a whole 2x2x4 slice. The times are simulated.
32 devices in a mesh: sp: 8 (over z, y), tp: 4 (over x, core).
Axes of the slice: x: 2, y: 2, z: 4, core: 2. Of those that a mesh axis runs over, the one named last changes fastest.
Arguments:
- latent: bfloat16 [1024, 2048], P(('sp', 'tp')), may hold values from -6 to 6
- context: bfloat16 [512, 2048], replicated, may hold values from -6 to 6
- condition: float32 [2048], replicated, may hold values from -6 to 6
- context_condition: float32 [2048], replicated, may hold values from -6 to 6
- modulation_weight: bfloat16 [2048, 3, 2048], P('sp', None, 'tp'), may hold values from -0.25 to 0.25
- norm_gain: float32 [2048], replicated, may hold values from 0.1 to 1.9
- gate_weight: bfloat16 [2048, 1024], P(None, 'tp'), may hold values from -0.125 to 0.125
- value_weight: bfloat16 [2048, 1024], P(None, 'tp'), may hold values from -0.125 to 0.125
- write_weight: bfloat16 [2048, 512], P(None, 'tp'), may hold values from -0.125 to 0.125
- read_weight: bfloat16 [2048, 512], P(None, 'tp'), may hold values from -0.125 to 0.125
- step_weight: bfloat16 [2048, 2, 16], replicated, may hold values from -0.125 to 0.125
- value_taps: bfloat16 [3, 1024], P(None, 'tp'), may hold values from -3.5 to 3.5
- map_taps: bfloat16 [3, 2, 512], P(None, None, 'tp'), may hold values from -3.5 to 3.5
- decay_rate: float32 [2, 16], replicated, may hold values from 1e-06 to 0.06
- decay_jump: float32 [2, 16, 1024], P(None, 'tp', 'sp'), may hold values from -2.76 to 0
- skip_gain: float32 [16], replicated, may hold values from 1 to 16
- group_gain: float32 [1024], P('tp'), may hold values from 0.1 to 1.9
- output_weight: bfloat16 [1024, 2048], P('tp'), may hold values from -0.1875 to 0.1875
- post_gain: float32 [2048], replicated, may hold values from 0.1 to 1.9
Outputs:
- updated: bfloat16 [1024, 2048], P(('sp', 'tp'))
All inputs are finite; a program needn't handle non-finite values.
Results may differ from a plain program's by a relative error of at most 0.014.
Values may be sent and summed in bfloat16 or wider, within the bound.
A program may use at most 64 MiB of HBM per device.

v0:
```python
import jax
import jax.numpy as jnp
from jax import lax
from jax.sharding import PartitionSpec as P

HEAD_DIM = 64
STATE = 64
SPAN = 128


EPSILON = 1e-06
HIGHEST = lax.Precision.HIGHEST


def carried_in_2(shard, axis, combine, identity, reverse):
    size, mine = (lax.axis_size(axis), lax.axis_index(axis))
    everything = jax.tree.map(
        lambda part, kind: lax.all_gather(part.astype(kind), axis),
        shard,
        jax.tree.map(lambda a: jnp.bfloat16 if a.dtype == jnp.float32 else a.dtype, shard),
    )
    start = jax.tree.map(
        lambda part, zero: jnp.broadcast_to(jnp.asarray(zero, part.dtype), part.shape),
        shard,
        identity,
    )

    def turn(k, before):
        at = size - 1 - k if reverse else k
        reached = at > mine if reverse else at < mine
        new = combine(
            before, jax.tree.map(lambda part, own: part[at].astype(own.dtype), everything, shard)
        )
        return jax.tree.map(lambda a, b: jnp.where(reached, a, b), new, before)

    return lax.fori_loop(0, size, turn, start)


def with_halo(cells, sides, width):
    for axis, dim in sides:
        count = lax.axis_size(axis)
        ends = count - 1
        head = lax.slice_in_dim(cells, 0, width, axis=dim)
        tail = lax.slice_in_dim(cells, cells.shape[dim] - width, cells.shape[dim], axis=dim)
        cells = jnp.concatenate(
            [
                lax.ppermute(tail, axis, [(i, (i + 1) % count) for i in range(ends)]),
                cells,
                lax.ppermute(head, axis, [((i + 1) % count, i) for i in range(ends)]),
            ],
            axis=dim,
        )
    return cells


def modulated_norm(row_block, gain_vec, shift_vec, scale_vec):
    widened = row_block.astype(jnp.float32)
    normed = widened * lax.rsqrt(jnp.mean(widened * widened, axis=-1, keepdims=True) + EPSILON)
    return (normed * gain_vec * (1.0 + scale_vec) + shift_vec).astype(jnp.bfloat16)


def short_conv(padded, conv_taps):
    length = padded.shape[0] - 2
    widened = padded.astype(jnp.float32)
    weights = conv_taps.astype(jnp.float32)
    summed = (
        weights[0] * widened[:length]
        + weights[1] * widened[1 : length + 1]
        + weights[2] * widened[2:]
    )
    return jax.nn.silu(summed)


def zero_rim(tensor):
    return jnp.pad(tensor, ((1, 1), (0, 0)))


def project(row_block, weight):
    return jnp.dot(row_block, weight, preferred_element_type=jnp.float32).astype(jnp.bfloat16)


def flip_rows(tensor, direction):
    if direction == 1:
        return jnp.flip(tensor, axis=0)
    return tensor


def sweep(inputs, step_sizes, log_decay, write_maps, read_maps, start_state):
    length, head_count, head_width = inputs.shape
    blocks = length // SPAN
    lower_mask = (jnp.arange(SPAN)[:, None] >= jnp.arange(SPAN)[None, :])[:, :, None]

    def cut_blocks(tensor):
        return tensor.reshape((blocks, SPAN) + tensor.shape[1:])

    def advance(carry_state, block_data):
        value_block, size_block, decay_block, write_block, read_block = block_data
        within = jnp.cumsum(decay_block, axis=0)
        weighted = value_block * size_block[:, :, None]
        log_gaps = jnp.where(lower_mask, within[:, None, :] - within[None, :, :], 0.0)
        fading = jnp.where(lower_mask, jnp.exp(log_gaps), 0.0)
        scores = jnp.einsum("ihn,jhn->ijh", read_block, write_block, precision=HIGHEST) * fading
        inner_term = jnp.einsum("ijh,jhp->ihp", scores, weighted, precision=HIGHEST)
        carried = jnp.einsum(
            "ihn,hpn->ihp", read_block * jnp.exp(within)[:, :, None], carry_state, precision=HIGHEST
        )
        block_total = within[-1]
        fresh_state = jnp.einsum(
            "jhn,jhp->hpn",
            write_block * jnp.exp(block_total[None, :] - within)[:, :, None],
            weighted,
            precision=HIGHEST,
        )
        return (
            jnp.exp(block_total)[:, None, None] * carry_state + fresh_state,
            inner_term + carried,
        )

    final_state, outputs = lax.scan(
        advance,
        start_state,
        (
            cut_blocks(inputs),
            cut_blocks(step_sizes),
            cut_blocks(log_decay),
            cut_blocks(write_maps),
            cut_blocks(read_maps),
        ),
    )
    return (outputs.reshape(length, head_count, head_width), final_state)


def chain_join(earlier, later):
    return (earlier[0] + later[0], jnp.exp(later[0])[:, None, None] * earlier[1] + later[1])


def carried_in(direction, element, identity):
    if direction == 0:
        return carried_in_2(element, "sp", chain_join, identity, False)
    return carried_in_2(element, "sp", chain_join, identity, True)


def body(
    latent,
    context,
    condition,
    context_condition,
    modulation_weight,
    norm_gain,
    gate_weight,
    value_weight,
    write_weight,
    read_weight,
    step_weight,
    value_taps,
    map_taps,
    decay_rate,
    decay_jump,
    skip_gain,
    group_gain,
    output_weight,
    post_gain,
):
    head_devices = lax.axis_size("tp")
    head_rank = lax.axis_index("tp")
    token_rank = lax.axis_index("sp")
    model_width = norm_gain.shape[0]
    own_rows = modulation_weight.shape[0]
    head_local = value_weight.shape[1] // HEAD_DIM
    group_local = write_weight.shape[1] // STATE
    conditions = jax.nn.silu(jnp.stack([condition, context_condition]))
    own_conditions = lax.dynamic_slice_in_dim(conditions, token_rank * own_rows, own_rows, 1)
    partial_value = jnp.einsum(
        "sd,dkc->skc", own_conditions, modulation_weight.astype(jnp.float32), precision=HIGHEST
    )
    column_share = partial_value.shape[2]
    placed = jnp.zeros((2, 3, head_devices, column_share), jnp.float32)
    placed = lax.dynamic_update_slice(placed, partial_value[:, :, None, :], (0, 0, head_rank, 0))
    modulation = lax.psum(placed, ("sp", "tp")).reshape(2, 3, model_width)
    head_start = head_rank * head_local
    rate_local = lax.dynamic_slice_in_dim(decay_rate, head_start, head_local, 1)
    skip_local = lax.dynamic_slice_in_dim(skip_gain, head_start, head_local, 0)
    own_step = lax.dynamic_slice_in_dim(step_weight, head_start, head_local, 2).reshape(
        model_width, 2 * head_local
    )
    normed = modulated_norm(latent, norm_gain, modulation[0, 0], modulation[0, 1])
    gathered = lax.all_gather(normed, "tp", axis=0, tiled=True)
    token_count = gathered.shape[0]
    gate_linear = project(gathered, gate_weight)
    step_linear = project(gathered, own_step).reshape(token_count, 2, head_local)
    joined = jnp.concatenate(
        [
            project(gathered, value_weight),
            project(gathered, write_weight),
            project(gathered, read_weight),
        ],
        axis=1,
    )
    padded = with_halo(joined, (("sp", 0),), 1)
    conv_taps = jnp.concatenate([value_taps, map_taps.reshape(3, -1)], axis=1)
    convolved = short_conv(padded, conv_taps)
    value_width = head_local * HEAD_DIM
    map_width = group_local * STATE
    repeat_count = head_local // group_local
    latent_values = convolved[:, :value_width].reshape(token_count, head_local, HEAD_DIM)
    latent_write = jnp.repeat(
        convolved[:, value_width : value_width + map_width].reshape(
            token_count, group_local, STATE
        ),
        repeat_count,
        axis=1,
    )
    latent_read = jnp.repeat(
        convolved[:, value_width + map_width :].reshape(token_count, group_local, STATE),
        repeat_count,
        axis=1,
    )
    normed_context = modulated_norm(context, norm_gain, modulation[1, 0], modulation[1, 1])
    context_value = project(normed_context, value_weight)
    context_map = project(normed_context, write_weight)
    context_step = project(normed_context, own_step)
    context_length = context_value.shape[0]
    context_values = short_conv(zero_rim(context_value), value_taps).reshape(
        context_length, head_local, HEAD_DIM
    )
    context_write = short_conv(zero_rim(context_map), map_taps[:, 0]).reshape(
        context_length, group_local, STATE
    )
    context_write = jnp.repeat(context_write, repeat_count, axis=1)
    context_step = context_step.reshape(context_length, 2, head_local)
    mixer_sum = skip_local[None, :, None] * latent_values
    identity = (
        jnp.zeros((head_local,), jnp.float32),
        jnp.zeros((head_local, HEAD_DIM, STATE), jnp.float32),
    )
    for direction in range(2):
        rate_head = rate_local[direction]
        latent_size = jax.nn.softplus(step_linear[:, direction].astype(jnp.float32))
        latent_decay = -latent_size * rate_head[None, :] + decay_jump[direction].T
        context_size = jax.nn.softplus(context_step[:, direction].astype(jnp.float32))
        context_decay = -context_size * rate_head[None, :]
        unused_rows, context_state = sweep(
            flip_rows(context_values, direction),
            flip_rows(context_size, direction),
            flip_rows(context_decay, direction),
            flip_rows(context_write, direction),
            flip_rows(context_write, direction),
            identity[1],
        )
        oriented_decay = flip_rows(latent_decay, direction)
        swept_rows, local_state = sweep(
            flip_rows(latent_values, direction),
            flip_rows(latent_size, direction),
            oriented_decay,
            flip_rows(latent_write, direction),
            flip_rows(latent_read, direction),
            identity[1],
        )
        cumulative = jnp.cumsum(oriented_decay, axis=0)
        before_log, before_state = carried_in(direction, (cumulative[-1], local_state), identity)
        entering = before_state + jnp.exp(before_log)[:, None, None] * context_state
        carried = jnp.einsum(
            "ihn,hpn->ihp",
            flip_rows(latent_read, direction) * jnp.exp(cumulative)[:, :, None],
            entering,
            precision=HIGHEST,
        )
        mixer_sum = mixer_sum + flip_rows(swept_rows + carried, direction)
    gated_rows = mixer_sum.reshape(token_count, value_width) * jax.nn.silu(
        gate_linear.astype(jnp.float32)
    )
    grouped = gated_rows.reshape(token_count, group_local, value_width // group_local)
    grouped = (
        grouped
        * lax.rsqrt(jnp.mean(grouped * grouped, axis=-1, keepdims=True) + EPSILON)
        * group_gain.reshape(group_local, value_width // group_local)
    )
    gated_rows = grouped.reshape(token_count, value_width).astype(jnp.bfloat16)
    mixed_rows = lax.psum_scatter(
        jnp.dot(gated_rows, output_weight, preferred_element_type=jnp.float32).astype(jnp.bfloat16),
        "tp",
        scatter_dimension=0,
        tiled=True,
    ).astype(jnp.float32)
    normed_out = (
        mixed_rows
        * lax.rsqrt(jnp.mean(mixed_rows * mixed_rows, axis=-1, keepdims=True) + EPSILON)
        * post_gain
    )
    return (latent.astype(jnp.float32) + modulation[0, 2] * normed_out).astype(jnp.bfloat16)


def solution(mesh):
    placed = (
        P(("sp", "tp"), None),
        P(),
        P(),
        P(),
        P("sp", None, "tp"),
        P(),
        P(None, "tp"),
        P(None, "tp"),
        P(None, "tp"),
        P(None, "tp"),
        P(),
        P(None, "tp"),
        P(None, None, "tp"),
        P(),
        P(None, "tp", "sp"),
        P(),
        P("tp"),
        P("tp", None),
        P(),
    )
    return jax.shard_map(
        body, mesh=mesh, in_specs=placed, out_specs=P(("sp", "tp"), None), check_vma=False
    )
```

profile of v0, /device:TPU:0, one launch (start us, length us, event | category | flops | bytes accessed | tf_op | source)
XLA Modules:
  0.0 261.5 jit_solution(11595066028982531883)
XLA Ops:
  6.5 1.8 convolution_bitcast_fusion.2
  8.5 42.4 %psum.7 = f32[2,3,2048]{2,0,1:T(2,128)S(1)} all-reduce(f32[2,3,2048]{2,0,1:T(2,128)S(1)} %reshape.310), channel_id=1, replica_groups=mesh['sp'=8,'tp'=4] {'sp','tp'}, use_global_device_ids=true, to_apply=%region_0.1 | all-reduce | flops 12288 | bytes 98304 | tf_op jit(solution)/shard_map/psum | solution.py:179
  53.7 7.9 %all_gather.23 = bf16[128,2048]{1,0:T(8,128)(2,1)S(1)} all-gather(bf16[32,2048]{1,0:T(8,128)(2,1)S(1)} %fusion.38), channel_id=1, replica_groups=mesh['sp'=8,'tp'=4] {'tp'}, dimensions={0}, use_global_device_ids=true | all-gather | bytes 655360 | tf_op jit(solution)/shard_map/all_gather | solution.py:187
  63.1 3.4 %collective-permute-start = (bf16[1,512]{1,0:T(2,128)(2,1)}, bf16[1,512]{1,0:T(2,128)(2,1)}, u32[]{:S(2)}, u32[]{:S(2)}) collective-permute-start(bf16[1,512]{1,0:T(2,128)(2,1)} %get-tuple-element.648), channel_id=1, source_target_pairs={{0,4},{4,8},{8,12},{12,16},{16,20},{20,24},{24,28},{1,5},{5,9},{9,... | collective-permute-start | bytes 3080 | tf_op jit(solution)/shard_map/ppermute | solution.py:47
  67.8 2.2 fusion.13
  70.9 1.4 convolution_convert_fusion.1
  72.3 1.4 convolution_convert_fusion.2
  74.7 2.2 convolution_convert_fusion.7
  88.5 7.4 %while.67 = (s32[]{:T(128)}, f32[4,64,64]{2,1,0:T(8,128)S(1)}, f32[4,128,4]{1,2,0:T(4,128)S(1)}, f32[4,128,4,64]{1,3,2,0:T(8,128)}, f32[4,128,4]{1,2,0:T(4,128)S...) while((s32[]{:T(128)}, f32[4,64,64]{2,1,0:T(8,128)S(1)}, ...), condition=%wide.region_8.9_spmd.clone, body=%wide.region_6.8_spmd.clone.sunk | while | flops 25346052 | bytes 684759 | solution.py:119
  97.8 1.6 rev.42
  99.4 3.4 %rev.41 = f32[512,4,64]{0,2,1:T(8,128)} reverse(f32[512,4,64]{0,2,1:T(8,128)} %bitcast.243), dimensions={0} | reverse | bytes 1048576 | tf_op jit(solution)/shard_map/jit(_flip)/rev | solution.py:84
  104.0 1.7 rev.43
  105.7 2.0 reshape.324
  107.7 8.1 %while.69 = (s32[]{:T(128)}, f32[4,64,64]{2,1,0:T(8,128)S(1)}, f32[4,128,4]{2,1,0:T(8,128)S(1)}, f32[4,128,4,64]{1,0,3,2:T(4,128)S(1)}, f32[4,128,4]{1,2,0:T(4,1...) while((s32[]{:T(128)}, f32[4,64,64]{2,1,0:T(8,128)S(1)}, ...), condition=%wide.region_14.15_spmd.clone, body=%wide.region_12.14_spmd.clone.sunk | while | flops 25346052 | bytes 942295 | solution.py:119
  108.0 1.3 constant_dynamic-slice_fusion.13
  112.1 1.3 constant_dynamic-slice_fusion.13
  114.1 1.3 constant_dynamic-slice_fusion.13
  116.6 20.7 %all-gather.2 = bf16[8,1,4]{2,1,0:T(2,128)(2,1)S(1)} all-gather(bf16[1,1,4]{2,1,0:T(2,128)(2,1)} %convert_bitcast_fusion.1), channel_id=1, replica_groups=mesh['sp'=8,'tp'=4] {'sp'}, dimensions={0}, use_global_device_ids=true | all-gather | bytes 72 | tf_op jit(solution)/shard_map/all_gather | solution.py:18
  137.2 16.4 %all-gather.3 = bf16[8,1,4]{2,1,0:T(2,128)(2,1)S(1)} all-gather(bf16[1,1,4]{2,1,0:T(2,128)(2,1)} %convert_bitcast_fusion), channel_id=1, replica_groups=mesh['sp'=8,'tp'=4] {'sp'}, dimensions={0}, use_global_device_ids=true | all-gather | bytes 72 | tf_op jit(solution)/shard_map/all_gather | solution.py:18
  159.2 31.2 %all-gather = bf16[32,64,64]{2,1,0:T(8,128)(2,1)S(1)} all-gather(bf16[4,64,64]{2,1,0:T(8,128)(2,1)S(1)} %fusion.26), channel_id=2, replica_groups=mesh['sp'=8,'tp'=4] {'sp'}, dimensions={0}, use_global_device_ids=true | all-gather | bytes 294912 | tf_op jit(solution)/shard_map/all_gather | solution.py:18
  192.0 31.7 %all-gather.1 = bf16[32,64,64]{2,1,0:T(8,128)(2,1)S(1)} all-gather(bf16[4,64,64]{2,1,0:T(8,128)(2,1)S(1)} %fusion.27), channel_id=3, replica_groups=mesh['sp'=8,'tp'=4] {'sp'}, dimensions={0}, use_global_device_ids=true | all-gather | bytes 294912 | tf_op jit(solution)/shard_map/all_gather | solution.py:18
  228.4 1.6 fusion.113
  231.6 20.2 %reduce-scatter.2.cloned.1.call-done = bf16[32,2048]{1,0:T(8,128)(2,1)} async-done(((bf16[128,2048]{1,0:T(8,128)(2,1)}), bf16[32,2048]{1,0:T(8,128)(2,1)}) %reduce-scatter.2.cloned.1.call-update) | async-done | bytes 131088 | tf_op jit(solution)/shard_map/reduce_scatter | solution.py:279
  252.9 1.7 fusion.39
  (282 shorter events, 49.7 us)
Async XLA Ops:
  6.5 223.9 %copy-start = (bf16[256,2048]{1,0:T(8,128)(2,1)S(1)}, bf16[256,2048]{1,0:T(8,128)(2,1)}, u32[]{:S(2)}) copy-start(bf16[256,2048]{1,0:T(8,128)(2,1)} %param.44) | copy-start | bytes 3145732
  6.5 55.0 %copy-start.5 = (bf16[2048,256]{1,0:T(8,128)(2,1)S(1)}, bf16[2048,256]{1,0:T(8,128)(2,1)}, u32[]{:S(2)}) copy-start(bf16[2048,256]{1,0:T(8,128)(2,1)} %param.34) | copy-start | bytes 3145732
  6.5 245.3 %reduce-scatter.2.cloned.1.call-start = ((), (), s32[]{:S(2)}) async-start(), calls=%async_computation.1 | async-start | bytes 655360 | tf_op jit(solution)/shard_map/reduce_scatter | solution.py:279
  8.3 53.9 %copy-start.3 = (bf16[2048,128]{1,0:T(8,128)(2,1)S(1)}, bf16[2048,128]{1,0:T(8,128)(2,1)}, u32[]{:S(2)}) copy-start(bf16[2048,128]{1,0:T(8,128)(2,1)} %param.35) | copy-start | bytes 1572868
  50.9 10.9 %copy-start.8 = (bf16[2048,128]{1,0:T(8,128)(2,1)S(1)}, bf16[2048,128]{1,0:T(8,128)(2,1)}, u32[]{:S(2)}) copy-start(bf16[2048,128]{1,0:T(8,128)(2,1)} %param.36) | copy-start | bytes 1572868
  61.9 8.1 %copy-start.16 = (f32[2048]{0:T(1024)S(1)}, f32[2048]{0:T(1024)}, u32[]{:S(2)}) copy-start(f32[2048]{0:T(1024)} %param.32) | copy-start | bytes 24580
  62.2 8.7 %copy-start.9 = (bf16[128,128]{1,0:T(8,128)(2,1)}, bf16[128,128]{1,0:T(8,128)(2,1)S(1)}, u32[]{:S(2)}) copy-start(bf16[128,128]{1,0:T(8,128)(2,1)S(1)} %convolution_convert_fusion.5) | copy-start | bytes 98308
  62.5 8.4 %copy-start.11 = (bf16[128,128]{1,0:T(8,128)(2,1)}, bf16[128,128]{1,0:T(8,128)(2,1)S(1)}, u32[]{:S(2)}) copy-start(bf16[128,128]{1,0:T(8,128)(2,1)S(1)} %convolution_convert_fusion.6) | copy-start | bytes 98308
  63.1 93.7 %collective-permute-start = (bf16[1,512]{1,0:T(2,128)(2,1)}, bf16[1,512]{1,0:T(2,128)(2,1)}, u32[]{:S(2)}, u32[]{:S(2)}) collective-permute-start(bf16[1,512]{1,0:T(2,128)(2,1)} %get-tuple-element.648), channel_id=1, source_target_pairs={{0,4},{4,8},{8,12},{12,16},{16,20},{20,24},{24,28},{1,5},{5,9},{9,... | collective-permute-start | bytes 3080 | tf_op jit(solution)/shard_map/ppermute | solution.py:47
  66.5 90.4 %collective-permute-start.1 = (bf16[1,512]{1,0:T(2,128)(2,1)}, bf16[1,512]{1,0:T(2,128)(2,1)}, u32[]{:S(2)}, u32[]{:S(2)}) collective-permute-start(bf16[1,512]{1,0:T(2,128)(2,1)} %get-tuple-element.649), channel_id=1, source_target_pairs={{4,0},{8,4},{12,8},{16,12},{20,16},{24,20},{28,24},{5,1},{9,5},{13... | collective-permute-start | bytes 3080 | tf_op jit(solution)/shard_map/ppermute | solution.py:49
  88.5 8.2 %copy-start.25 = (bf16[3,2,128]{2,1,0:T(2,128)(2,1)S(1)}, bf16[3,2,128]{2,1,0:T(2,128)(2,1)}, u32[]{:S(2)}) copy-start(bf16[3,2,128]{2,1,0:T(2,128)(2,1)} %param.39) | copy-start | bytes 4612
  88.5 8.2 %copy-start.22 = (bf16[3,256]{1,0:T(4,128)(2,1)S(1)}, bf16[3,256]{1,0:T(4,128)(2,1)}, u32[]{:S(2)}) copy-start(bf16[3,256]{1,0:T(4,128)(2,1)} %param.38) | copy-start | bytes 4612
  88.5 8.7 %copy-start.18 = (f32[512,4]{0,1:T(4,128)S(1)}, f32[512,4]{0,1:T(4,128)}, u32[]{:S(2)}) copy-start(f32[512,4]{0,1:T(4,128)} %get-tuple-element.662) | copy-start | bytes 24580
  107.7 47.2 %copy-start.14 = (f32[128,4]{1,0:T(8,128)S(1)}, f32[128,4]{1,0:T(8,128)}, u32[]{:S(2)}) copy-start(f32[128,4]{1,0:T(8,128)} %get-tuple-element.650) | copy-start | bytes 6148
  107.7 49.1 %copy-start.10 = (bf16[128,128]{1,0:T(8,128)(2,1)S(1)}, bf16[128,128]{1,0:T(8,128)(2,1)}, u32[]{:S(2)}) copy-start(bf16[128,128]{1,0:T(8,128)(2,1)} %copy-done.9) | copy-start | bytes 98308
  107.7 49.1 %copy-start.12 = (bf16[128,128]{1,0:T(8,128)(2,1)S(1)}, bf16[128,128]{1,0:T(8,128)(2,1)}, u32[]{:S(2)}) copy-start(bf16[128,128]{1,0:T(8,128)(2,1)} %copy-done.11) | copy-start | bytes 98308
  115.8 43.0 %copy-start.19 = (f32[128,4]{0,1:T(4,128)S(1)}, f32[128,4]{0,1:T(4,128)}, u32[]{:S(2)}) copy-start(f32[128,4]{0,1:T(4,128)} %get-tuple-element.668) | copy-start | bytes 6148
  115.9 43.0 %copy-start.30 = (f32[4]{0:T(128)S(1)}, f32[4]{0:T(128)}, u32[]{:S(2)}) copy-start(f32[4]{0:T(128)} %exponential_multiply_fusion.1) | copy-start | bytes 52
  155.0 35.5 %copy-start.20 = (f32[4]{0:T(128)S(1)}, f32[4]{0:T(128)}, u32[]{:S(2)}) copy-start(f32[4]{0:T(128)} %custom-call) | copy-start | bytes 52
  158.4 33.2 %copy-start.29 = (f32[4]{0:T(128)S(1)}, f32[4]{0:T(128)}, u32[]{:S(2)}) copy-start(f32[4]{0:T(128)} %exponential_multiply_fusion) | copy-start | bytes 52
  191.5 33.7 %copy-start.15 = (pred[128,128]{0,1:T(8,128)(4,1)S(1)}, pred[128,128]{0,1:T(8,128)(4,1)}, u32[]{:S(2)}) copy-start(pred[128,128]{0,1:T(8,128)(4,1)} %iota_compare_fusion) | copy-start | bytes 49156
  229.9 23.0 %copy-start.4 = (bf16[32,2048]{1,0:T(8,128)(2,1)S(1)}, bf16[32,2048]{1,0:T(8,128)(2,1)}, u32[]{:S(2)}) copy-start(bf16[32,2048]{1,0:T(8,128)(2,1)} %param.27) | copy-start | bytes 393220
  229.9 23.0 %copy-start.17 = (f32[1,1,2048]{2,0,1:T(1,128)S(1)}, f32[1,1,2048]{2,0,1:T(1,128)}, u32[]{:S(2)}) copy-start(f32[1,1,2048]{2,0,1:T(1,128)} %get-tuple-element.654) | copy-start | bytes 24580
  229.9 23.0 %copy-start.23 = (f32[2048]{0:T(1024)S(1)}, f32[2048]{0:T(1024)}, u32[]{:S(2)}) copy-start(f32[2048]{0:T(1024)} %param.45) | copy-start | bytes 24580
  (11 other events, 49.4 us)
Sparse Core Ops, SparseCore 0:
  231.8 20.0 reduce-scatter.1
where the time goes:
time: 263 us; the launch traced here: 261 us
  blocking collectives  150 us (57%)
  local copies, waits for them, and re-layouts  29.5 us (11%)
  other arithmetic  20.9 us (8%)
  matrix products  20.8 us (8%)
  waiting for transfers between devices  20.2 us (8%)
  between operations  14.2 us (5%)
  starting transfers between devices  4.64 us (2%)
    all_gather x4, blocking collectives, carried_in_2(): lax.all_gather(part.astype(kind), axis)  100 us
    psum x1, blocking collectives, body(): modulation = lax.psum(placed, ('sp', 'tp')).reshape(2, 3, model_width)  42.4 us
    reduce_scatter x1, waiting for transfers between devices, body(): lax.psum_scatter(jnp.dot(gated_rows, output_weight, preferred_element_typ...  20.2 us
    rev x12, local copies, waits for them, and re-layouts, flip_rows(): return jnp.flip(tensor, axis=0)  9.24 us
    all_gather x1, blocking collectives, body(): gathered = lax.all_gather(normed, 'tp', axis=0, tiled=True)  7.89 us
    dot_general x8, matrix products, project(): jnp.dot(row_block, weight, preferred_element_type=jnp.float32)  7.73 us
    dot_general x10, matrix products, advance(): jnp.einsum('jhn,jhp->hpn', write_block * jnp.exp(block_total[None, :] - w...  7.06 us
    dynamic_slice x16, local copies, waits for them, and re-layouts, sweep(): lax.scan(advance, start_state, (cut_blocks(inputs), cut_blocks(step_sizes...  6.44 us
  transfers between devices with their start and end apart: 3, of which 1 were waited for; matrix products, arithmetic and copies ran while one was open for 20% of the time, Pallas kernels for 0%

commit v1 on v0

v1 whole, which is shorter than its diff:
```python
import functools

import jax
import jax.numpy as jnp
from jax import lax
from jax.experimental import pallas as pl
from jax.experimental.pallas import tpu as pltpu
from jax.sharding import PartitionSpec as P

HEAD_DIM = 64
STATE = 64
EPSILON = 1e-06
HIGHEST = lax.Precision.HIGHEST
MESH = pl.DeviceIdType.MESH
EDGE = 16
CHUNK = 128
F32 = jnp.float32
BF16 = jnp.bfloat16


def silu(x):
    return x / (1.0 + jnp.exp(-x))


def softplus(x):
    return jnp.maximum(x, 0.0) + jnp.log1p(jnp.exp(-jnp.abs(x)))


def mask_of(shape, rule):
    rows = lax.broadcasted_iota(jnp.int32, shape, 0)
    cols = lax.broadcasted_iota(jnp.int32, shape, 1)
    return rule(rows, cols)


def tri_of(size, rule):
    return jnp.where(mask_of((size, size), rule), 1.0, 0.0).astype(F32)


def dot32(a, b):
    return jnp.dot(a, b, precision=HIGHEST, preferred_element_type=F32)


def dotf(a, b):
    return jnp.dot(a, b, preferred_element_type=F32)


def dot_nt(a, b):
    return lax.dot_general(a, b, (((1,), (1,)), ((), ())), preferred_element_type=F32)


def columns_of(rows8):
    have = rows8.shape[0]
    pad = jnp.zeros((CHUNK - have, CHUNK), F32)
    return jnp.concatenate([rows8, pad], axis=0).T


def stats_pass(src, dst, count):
    @pl.loop(0, count // 16)
    def _(i):
        at = pl.ds(pl.multiple_of(i * 16, 16), 16)
        x = src[at, :].astype(F32)
        inv = lax.rsqrt(jnp.mean(x * x, axis=-1, keepdims=True) + EPSILON)
        dst[at, :] = jnp.broadcast_to(inv, (16, 128))


def norm_pass(src, stat, dst, src_at, dst_at, count, gain, shift):
    lanes = src.shape[1] // 128

    @pl.loop(0, count // 16)
    def _(i):
        at = pl.ds(pl.multiple_of(src_at + i * 16, 16), 16)
        to = pl.ds(pl.multiple_of(dst_at + i * 16, 16), 16)
        inv = jnp.concatenate([stat[at, :]] * lanes, axis=1)
        dst[to, :] = (src[at, :].astype(F32) * inv * gain + shift).astype(BF16)


def kernel(
    part, latent, context_hbm, norm_gain, post_gain, gate_hbm, value_hbm, write_hbm, read_hbm,
    step, taps, rate, jump, skip, group_gain, output_hbm,
    out,
    context, gate_w, value_w, write_w, read_w, output_w,
    xbuf, xstat, cstat, hbuf, chid, ubuf, ucbuf, cstep,
    part_a, modbuf, stbuf, strecv, obuf, rbuf, state_c,
    load_sem, own_sem, xs_sem, xr_sem, hs_sem, hr_sem, as_sem, ar_sem, bs_sem, br_sem,
    ss_sem, sr_sem, os_sem, or_sem,
    *, n_sp, n_tp,
):
    sp, tp = lax.axis_index("sp"), lax.axis_index("tp")
    rows = latent.shape[0]
    tokens = n_tp * rows
    width = latent.shape[1]
    vwidth = value_w.shape[1]
    mwidth = write_w.shape[1]
    groups = mwidth // STATE
    heads = vwidth // HEAD_DIM
    per = heads // groups
    gwidth = vwidth // groups
    ctx = context.shape[0]
    col_chunks = obuf.shape[0]
    cwidth = obuf.shape[3]

    loads = [
        pltpu.make_async_copy(s, d, load_sem.at[i])
        for i, (s, d) in enumerate(
            (
                (context_hbm, context), (value_hbm, value_w), (write_hbm, write_w),
                (read_hbm, read_w), (gate_hbm, gate_w), (output_hbm, output_w),
            )
        )
    ]
    own_x = pltpu.make_async_copy(
        latent, xbuf.at[pl.ds(pl.multiple_of(EDGE + tp * rows, 16), rows)], own_sem
    )
    own_x.start()
    for c in loads:
        c.start()

    barrier = pltpu.get_barrier_semaphore()

    @pl.loop(1, n_sp)
    def _(r):
        pl.semaphore_signal(barrier, inc=1, device_id={"sp": lax.rem(sp + r, n_sp)}, device_id_type=MESH)

    for r in range(1, n_tp):
        pl.semaphore_signal(barrier, inc=1, device_id={"tp": lax.rem(tp + r, n_tp)}, device_id_type=MESH)
    pl.semaphore_wait(barrier, n_sp - 1 + n_tp - 1)

    def remote(src, dst, s, r, **where):
        return pltpu.make_async_remote_copy(
            src_ref=src, dst_ref=dst, send_sem=s, recv_sem=r, device_id=where, device_id_type=MESH
        )

    def send_a(r):
        peer = lax.rem(sp + r, n_sp)
        return remote(part, part_a.at[sp], as_sem.at[r], ar_sem.at[sp], sp=peer)

    def recv_a(r):
        peer = lax.rem(sp + r, n_sp)
        return remote(part, part_a.at[peer], as_sem.at[r], ar_sem.at[peer], sp=peer)

    @pl.loop(1, n_sp)
    def _(r):
        send_a(r).start()

    def x_rows(t):
        return xbuf.at[pl.ds(pl.multiple_of(EDGE + t * rows, 16), rows)]

    def send_x(r):
        return remote(latent, x_rows(tp), xs_sem.at[r], xr_sem.at[tp], tp=lax.rem(tp + r, n_tp))

    def recv_x(r):
        peer = lax.rem(tp + r, n_tp)
        return remote(latent, x_rows(peer), xs_sem.at[r], xr_sem.at[peer], tp=peer)

    for r in range(1, n_tp):
        send_x(r).start()

    loads[0].wait()
    stats_pass(context, cstat, ctx)

    total_mod = part[...]

    def add_a(r, acc):
        recv_a(r).wait_recv()
        return acc + part_a[lax.rem(sp + r, n_sp)]

    total_mod = lax.fori_loop(1, n_sp, add_a, total_mod)
    modbuf[tp] = total_mod

    def send_b(r):
        return remote(modbuf.at[tp], modbuf.at[tp], bs_sem.at[r], br_sem.at[tp], tp=lax.rem(tp + r, n_tp))

    def recv_b(r):
        peer = lax.rem(tp + r, n_tp)
        return remote(modbuf.at[peer], modbuf.at[peer], bs_sem.at[r], br_sem.at[peer], tp=peer)

    for r in range(1, n_tp):
        send_b(r).start()

    own_x.wait()
    for r in range(1, n_tp):
        recv_x(r).wait_recv()

    low = xbuf.at[pl.ds(0, EDGE)]
    high = xbuf.at[pl.ds(EDGE + tokens, EDGE)]
    first = xbuf.at[pl.ds(EDGE, EDGE)]
    last = xbuf.at[pl.ds(tokens, EDGE)]
    right = lax.rem(sp + 1, n_sp)
    left = lax.rem(sp + n_sp - 1, n_sp)
    to_right = remote(last, low, hs_sem.at[0], hr_sem.at[0], sp=right)
    to_left = remote(first, high, hs_sem.at[1], hr_sem.at[1], sp=left)
    has_right = sp < n_sp - 1
    has_left = sp > 0

    @pl.when(has_right)
    def _():
        to_right.start()

    @pl.when(has_left)
    def _():
        to_left.start()

    @pl.when(jnp.logical_not(has_left))
    def _():
        low[...] = jnp.zeros((EDGE, width), BF16)

    @pl.when(jnp.logical_not(has_right))
    def _():
        high[...] = jnp.zeros((EDGE, width), BF16)

    @pl.when(has_left)
    def _():
        to_right.wait_recv()

    @pl.when(has_right)
    def _():
        to_left.wait_recv()

    stats_pass(xbuf, xstat, tokens + 2 * EDGE)

    for r in range(1, n_tp):
        recv_b(r).wait_recv()
    mod = jnp.concatenate([modbuf[t] for t in range(n_tp)], axis=1)
    gain_l = norm_gain[...] * (1.0 + mod[1:2])
    shift_l = mod[0:1]
    gain_c = norm_gain[...] * (1.0 + mod[4:5])
    shift_c = mod[3:4]

    norm_pass(xbuf, xstat, hbuf, 0, 0, tokens + 2 * EDGE, gain_l, shift_l)

    for c in loads[1:5]:
        c.wait()
    hidden = hbuf[...]
    span = tokens + 2 * EDGE
    row_id = lax.broadcasted_iota(jnp.int32, (span, 1), 0)
    inside = jnp.logical_and(
        jnp.logical_or(row_id >= EDGE, has_left), jnp.logical_or(row_id < EDGE + tokens, has_right)
    )

    def rounded(x):
        return x.astype(BF16).astype(F32)

    ubuf[:, 0:vwidth] = jnp.where(inside, rounded(dotf(hidden, value_w[...])), 0.0)
    ubuf[:, vwidth : vwidth + mwidth] = jnp.where(inside, rounded(dotf(hidden, write_w[...])), 0.0)
    ubuf[:, vwidth + mwidth :] = jnp.where(inside, rounded(dotf(hidden, read_w[...])), 0.0)
    main = hbuf[EDGE : EDGE + tokens, :]

    def conv(ref, at, count, lo, hi, tap_lo):
        t = taps[:, tap_lo : tap_lo + hi - lo]
        return silu(
            t[0:1] * ref[pl.ds(at - 1, count), lo:hi]
            + t[1:2] * ref[pl.ds(at, count), lo:hi]
            + t[2:3] * ref[pl.ds(at + 1, count), lo:hi]
        )

    nrow = 2 * heads
    values = conv(ubuf, EDGE, tokens, 0, vwidth, 0)
    writes = conv(ubuf, EDGE, tokens, vwidth, vwidth + mwidth, vwidth)
    reads = conv(ubuf, EDGE, tokens, vwidth + mwidth, vwidth + 2 * mwidth, vwidth + mwidth)
    writes_b = writes.astype(BF16)
    reads_b = reads.astype(BF16)

    size = softplus(rounded(dot_nt(step[...], main)))[:nrow]
    decay = -size * rate[...] + jump[...]
    forward = lax.broadcasted_iota(jnp.int32, (nrow, 1), 0) < heads
    upto = tri_of(CHUNK, lambda k, i: k <= i)
    since = tri_of(CHUNK, lambda k, i: k >= i)
    after = tri_of(CHUNK, lambda k, i: k > i)
    before = tri_of(CHUNK, lambda k, i: k < i)
    cum = jnp.where(forward, dot32(decay, upto), dot32(decay, since))
    rest = jnp.where(forward, dot32(decay, after), dot32(decay, before))
    total = jnp.sum(decay, axis=1, keepdims=True)
    cols = columns_of(jnp.concatenate([cum, size * jnp.exp(rest), jnp.exp(cum)], axis=0))

    lane = lax.broadcasted_iota(jnp.int32, (1, gwidth), 1) // HEAD_DIM

    def by_head(pick, g):
        out_v = pick(g * per)
        for k in range(1, per):
            out_v = jnp.where(lane == k, pick(g * per + k), out_v)
        return out_v

    def states(write_t, vals, col_at, d):
        parts = []
        for g in range(groups):
            scale = by_head(lambda h: col_at(d * heads + h), g)
            scaled = (vals[:, g * gwidth : (g + 1) * gwidth] * scale).astype(BF16)
            parts.append(dotf(write_t, scaled)[g * STATE : (g + 1) * STATE])
        return jnp.concatenate(parts, axis=0)

    write_t = writes.T.astype(BF16)
    pad_rows = stbuf.shape[1] - mwidth - 2 * groups
    for d in range(2):
        st = states(write_t, values, lambda r: cols[:, nrow + r : nrow + r + 1], d)
        tot = jnp.concatenate(
            [by_head(lambda h: total[d * heads + h : d * heads + h + 1], g) for g in range(groups)], axis=0
        )
        tot_hi = tot.astype(BF16).astype(F32)
        extra = jnp.concatenate([tot_hi, tot - tot_hi, jnp.zeros((pad_rows, gwidth), F32)], axis=0)
        stbuf[d] = jnp.concatenate([st, extra], axis=0).astype(BF16)

    def send_s(d, k):
        return remote(stbuf.at[d], strecv.at[sp], ss_sem.at[k], sr_sem.at[sp], sp=k)

    def recv_s(k):
        return remote(stbuf.at[0], strecv.at[k], ss_sem.at[k], sr_sem.at[k], sp=k)

    @pl.loop(sp + 1, n_sp)
    def _(k):
        send_s(0, k).start()

    @pl.loop(0, sp)
    def _(k):
        send_s(1, k).start()

    pad8 = jnp.zeros((8, vwidth + mwidth), F32)
    ucbuf[0:8, :] = pad8
    ucbuf[8 + ctx : 16 + ctx, :] = pad8

    for i in range(ctx // CHUNK):
        norm_pass(context, cstat, chid, i * CHUNK, 0, CHUNK, gain_c, shift_c)
        hid = chid[...]
        ucbuf[8 + i * CHUNK : 8 + (i + 1) * CHUNK, 0:vwidth] = rounded(dotf(hid, value_w[...]))
        ucbuf[8 + i * CHUNK : 8 + (i + 1) * CHUNK, vwidth:] = rounded(dotf(hid, write_w[...]))
        cstep[i] = softplus(rounded(dot_nt(step[...], hid)))[:nrow]

    n_chunk = ctx // CHUNK
    decays = [-cstep[i] * rate[...] for i in range(n_chunk)]
    totals = [jnp.sum(a, axis=1, keepdims=True) for a in decays]
    entering = [None, None]
    for i in range(n_chunk):
        zero = jnp.zeros((nrow, 1), F32)
        later = sum(totals[i + 1 :], zero)
        earlier = sum(totals[:i], zero)
        rest_c = jnp.where(
            forward, dot32(decays[i], after) + later, dot32(decays[i], before) + earlier
        )
        ccols = columns_of(cstep[i] * jnp.exp(rest_c))
        cvals = conv(ucbuf, 8 + i * CHUNK, CHUNK, 0, vwidth, 0)
        cwrite_t = conv(ucbuf, 8 + i * CHUNK, CHUNK, vwidth, vwidth + mwidth, vwidth).T.astype(BF16)
        for d in range(2):
            st = states(cwrite_t, cvals, lambda r: ccols[:, r : r + 1], d)
            entering[d] = st if entering[d] is None else entering[d] + st

    ge = mask_of((tokens, tokens), lambda i, j: i >= j)
    le = mask_of((tokens, tokens), lambda i, j: i <= j)
    lane_m = lax.broadcasted_iota(jnp.int32, (1, mwidth), 1) // STATE
    inner = []
    for g in range(groups):
        own = jnp.where(lane_m == g, reads, 0.0).astype(BF16)
        score = dot_nt(own, writes_b)
        vg = values[:, g * gwidth : (g + 1) * gwidth].astype(BF16)
        made = []
        for k in range(per):
            h = g * per + k
            mix = jnp.zeros((tokens, tokens), F32)
            for d, keep in ((0, ge), (1, le)):
                r = d * heads + h
                gap = jnp.minimum(cols[:, r : r + 1] - cum[r : r + 1, :], 0.0)
                mix = mix + jnp.where(keep, jnp.exp(gap) * size[r : r + 1, :], 0.0)
            made.append(dotf((score * mix).astype(BF16), vg))
        inner.append(by_head(lambda h: made[h - g * per], g))
    mixer = skip[...] * values + jnp.concatenate(inner, axis=1)

    loads[5].wait()
    gate = silu(rounded(dotf(main, gate_w[...])))

    def join(k, state):
        recv_s(k).wait_recv()
        got = strecv[k].astype(F32)
        logs = got[mwidth : mwidth + groups] + got[mwidth + groups : mwidth + 2 * groups]
        fade = jnp.exp(logs)
        fade = jnp.concatenate(
            [jnp.broadcast_to(fade[g : g + 1], (STATE, gwidth)) for g in range(groups)], axis=0
        )
        return fade * state + got[:mwidth]

    entering[0] = lax.fori_loop(0, sp, join, entering[0])
    entering[1] = lax.fori_loop(0, n_sp - 1 - sp, lambda i, s: join(n_sp - 1 - i, s), entering[1])
    row_m = lax.broadcasted_iota(jnp.int32, (mwidth, 1), 0) // STATE
    for d in range(2):
        full = jnp.concatenate(
            [jnp.where(row_m == g, entering[d], 0.0) for g in range(groups)], axis=1
        ).astype(BF16)
        fade = jnp.concatenate(
            [
                by_head(lambda h: cols[:, 2 * nrow + d * heads + h : 2 * nrow + d * heads + h + 1], g)
                for g in range(groups)
            ],
            axis=1,
        )
        mixer = mixer + fade * dotf(reads_b, full)

    gated = mixer * gate
    pieces = []
    for g in range(groups):
        p = gated[:, g * gwidth : (g + 1) * gwidth]
        pieces.append(p * lax.rsqrt(jnp.mean(p * p, axis=-1, keepdims=True) + EPSILON))
    gated = (jnp.concatenate(pieces, axis=1) * group_gain[...]).astype(BF16)

    def send_o(c, r):
        peer = lax.rem(tp + r, n_tp)
        return remote(obuf.at[c, peer], rbuf.at[c, tp], os_sem.at[c, r], or_sem.at[c, tp], tp=peer)

    def recv_o(c, r):
        peer = lax.rem(tp + r, n_tp)
        return remote(obuf.at[c, peer], rbuf.at[c, peer], os_sem.at[c, r], or_sem.at[c, peer], tp=peer)

    for c in range(col_chunks):
        prod = dotf(gated, output_w[:, c * cwidth : (c + 1) * cwidth]).astype(BF16)
        for t in range(n_tp):
            obuf[c, t] = prod[t * rows : (t + 1) * rows]
        for r in range(1, n_tp):
            send_o(c, r).start()

    mixed = []
    for c in range(col_chunks):
        acc = obuf[c, tp].astype(F32)
        for r in range(1, n_tp):
            recv_o(c, r).wait_recv()
            acc = acc + rbuf[c, lax.rem(tp + r, n_tp)].astype(F32)
        mixed.append(acc)
    mixed = jnp.concatenate(mixed, axis=1)
    inv = lax.rsqrt(jnp.mean(mixed * mixed, axis=-1, keepdims=True) + EPSILON)
    gate_row = jnp.concatenate([modbuf[t, 2:3] for t in range(n_tp)], axis=1)
    out[...] = (latent[...].astype(F32) + gate_row * (mixed * inv * post_gain[...])).astype(BF16)

    @pl.loop(1, n_sp)
    def _(r):
        send_a(r).wait_send()

    for r in range(1, n_tp):
        send_x(r).wait_send()
        send_b(r).wait_send()

    @pl.when(has_right)
    def _():
        to_right.wait_send()

    @pl.when(has_left)
    def _():
        to_left.wait_send()

    @pl.loop(sp + 1, n_sp)
    def _(k):
        send_s(0, k).wait_send()

    @pl.loop(0, sp)
    def _(k):
        send_s(1, k).wait_send()

    for c in range(col_chunks):
        for r in range(1, n_tp):
            send_o(c, r).wait_send()


def body(
    latent, context, condition, context_condition, modulation_weight, norm_gain, gate_weight,
    value_weight, write_weight, read_weight, step_weight, value_taps, map_taps, decay_rate,
    decay_jump, skip_gain, group_gain, output_weight, post_gain,
):
    n_sp, n_tp = lax.axis_size("sp"), lax.axis_size("tp")
    sp, tp = lax.axis_index("sp"), lax.axis_index("tp")
    rows, width = latent.shape
    ctx = context.shape[0]
    vwidth, mwidth = value_weight.shape[1], write_weight.shape[1]
    heads, groups = vwidth // HEAD_DIM, mwidth // STATE
    gwidth = vwidth // groups
    tokens = rows * n_tp
    own_rows = modulation_weight.shape[0]
    share = modulation_weight.shape[2]
    conditions = jax.nn.silu(jnp.stack([condition, context_condition]))
    own = lax.dynamic_slice_in_dim(conditions, sp * own_rows, own_rows, 1)
    part = jnp.einsum("sd,dkc->skc", own, modulation_weight.astype(F32), precision=HIGHEST)
    part = jnp.pad(part.reshape(6, share), ((0, 2), (0, 0)))
    head_at = tp * heads
    nrow = 2 * heads
    step = lax.dynamic_slice_in_dim(step_weight, head_at, heads, 2)
    step = step.transpose(1, 2, 0).reshape(nrow, width)
    step = jnp.pad(step, ((0, -nrow % 16), (0, 0)))
    rate = lax.dynamic_slice_in_dim(decay_rate, head_at, heads, 1).reshape(nrow, 1)
    skip = jnp.repeat(lax.dynamic_slice_in_dim(skip_gain, head_at, heads, 0), HEAD_DIM).reshape(1, vwidth)
    taps = jnp.concatenate([value_taps, map_taps.reshape(3, -1)], axis=1).astype(F32)
    jump = decay_jump.reshape(nrow, tokens)
    chunks = 4
    cwidth = width // chunks
    srow = mwidth + 16
    vm = pltpu.VMEM
    dma = pltpu.SemaphoreType.DMA
    in_vmem = pl.BlockSpec(memory_space=pltpu.VMEM)
    in_any = pl.BlockSpec(memory_space=pl.ANY)
    return pl.pallas_call(
        functools.partial(kernel, n_sp=n_sp, n_tp=n_tp),
        out_shape=jax.ShapeDtypeStruct((rows, width), BF16),
        in_specs=[
            in_vmem, in_vmem, in_any, in_vmem, in_vmem, in_any, in_any, in_any, in_any,
            in_vmem, in_vmem, in_vmem, in_vmem, in_vmem, in_vmem, in_any,
        ],
        out_specs=in_vmem,
        scratch_shapes=[
            vm((ctx, width), BF16), vm((width, vwidth), BF16), vm((width, vwidth), BF16),
            vm((width, mwidth), BF16), vm((width, mwidth), BF16), vm((vwidth, width), BF16),
            vm((tokens + 2 * EDGE, width), BF16), vm((tokens + 2 * EDGE, 128), F32),
            vm((ctx, 128), F32), vm((tokens + 2 * EDGE, width), BF16), vm((CHUNK, width), BF16),
            vm((tokens + 2 * EDGE, vwidth + 2 * mwidth), F32), vm((ctx + 16, vwidth + mwidth), F32),
            vm((ctx // CHUNK, nrow, CHUNK), F32),
            vm((n_sp, 8, share), F32), vm((n_tp, 8, share), F32),
            vm((2, srow, gwidth), BF16), vm((n_sp, srow, gwidth), BF16),
            vm((chunks, n_tp, rows, cwidth), BF16), vm((chunks, n_tp, rows, cwidth), BF16),
            vm((2, mwidth, gwidth), F32),
            dma((6,)), dma, dma((n_tp,)), dma((n_tp,)), dma((2,)), dma((2,)),
            dma((n_sp,)), dma((n_sp,)), dma((n_tp,)), dma((n_tp,)), dma((n_sp,)), dma((n_sp,)),
            dma((chunks, n_tp)), dma((chunks, n_tp)),
        ],
        compiler_params=pltpu.CompilerParams(
            collective_id=0, has_side_effects=True, vmem_limit_bytes=48 * 1024 * 1024
        ),
    )(
        part, latent, context, norm_gain.reshape(1, -1), post_gain.reshape(1, -1), gate_weight,
        value_weight, write_weight, read_weight, step, taps, rate, jump, skip,
        group_gain.reshape(1, -1), output_weight,
    )


def solution(mesh):
    placed = (
        P(("sp", "tp"), None), P(), P(), P(), P("sp", None, "tp"), P(), P(None, "tp"), P(None, "tp"),
        P(None, "tp"), P(None, "tp"), P(), P(None, "tp"), P(None, None, "tp"), P(),
        P(None, "tp", "sp"), P(), P("tp"), P("tp", None), P(),
    )
    return jax.shard_map(
        body, mesh=mesh, in_specs=placed, out_specs=P(("sp", "tp"), None), check_vma=False
    )
```

time: 263 us -> 50.5 us (0.19)
  blocking collectives: 150 us -> 0 us
  Pallas kernels: 0 us -> 34.5 us
  other arithmetic: 20.9 us -> 0.69 us
  waiting for transfers between devices: 20.2 us -> 0 us
  matrix products: 20.8 us -> 1.17 us
  local copies, waits for them, and re-layouts: 29.5 us -> 13.4 us
  between operations: 14.2 us -> 0.06 us
  starting transfers between devices: 4.64 us -> 0 us
    all_gather x5 -> x0, blocking collectives: 108 us -> none  [the longest x4 100 us: carried_in_2(): lax.all_gather(part.astype(kind), axis)]
    psum x1 -> x0, blocking collectives: 42.4 us -> none  [body(): modulation = lax.psum(placed, ('sp', 'tp')).reshape(2, 3, model_width)]
    pallas_call x0 -> x1, Pallas kernels: none -> 34.5 us  [body(): pl.pallas_call(functools.partial(kernel, n_sp=n_sp, n_tp=n_tp), out_shape...]
    reduce_scatter x1 -> x0, waiting for transfers between devices: 20.2 us -> none  [body(): lax.psum_scatter(jnp.dot(gated_rows, output_weight, preferred_element_typ...]
    dot_general x28 -> x1, matrix products: 20.8 us -> 1.17 us  [body(): jnp.einsum('sd,dkc->skc', own, modulation_weight.astype(F32), precision=H...]
    rev x12 -> x0, local copies, waits for them, and re-layouts: 9.24 us -> none  [flip_rows(): return jnp.flip(tensor, axis=0)]
    unnamed x70 -> x24, local copies, waits for them, and re-layouts: 2.66 us -> 10.8 us
    dynamic_slice x19 -> x2, local copies, waits for them, and re-layouts: 8.19 us -> 1.55 us  [the longest x1 0.8 us: body(): lax.dynamic_slice_in_dim(skip_gain, head_at, heads, 0)]
  transfers between devices with their start and end apart: 3 -> 0, of which waited for: 1 -> 0; matrix products, arithmetic and copies ran while one was open for 20% -> 0% of each run, Pallas kernels for 0% -> 0%
where the time goes in v1:
time: 50.5 us; the launch traced here: 49.9 us
  Pallas kernels  34.5 us (68%)
  local copies, waits for them, and re-layouts  13.4 us (27%)
  matrix products  1.17 us (2%)
  other arithmetic  0.69 us (1%)
    pallas_call x1, Pallas kernels, body(): pl.pallas_call(functools.partial(kernel, n_sp=n_sp, n_tp=n_tp), out_shape...  34.5 us
    unnamed x24, local copies, waits for them, and re-layouts  10.8 us
    dot_general x1, matrix products, body(): jnp.einsum('sd,dkc->skc', own, modulation_weight.astype(F32), precision=H...  1.17 us

profile of v1, /device:TPU:0, one launch (start us, length us, event | category | flops | bytes accessed | tf_op | source)
XLA Modules:
  0.0 49.9 jit_solution(1270736521801523698)
XLA Ops:
  0.0 0.0 copy-start
  0.0 0.8 %dynamic_slice.15 = f32[4]{0:T(128)S(1)} dynamic-slice(f32[16]{0:T(128)} %param.34, s32[]{:T(128)S(6)} %select_n.9), dynamic_slice_sizes={4} | dynamic-slice | bytes 36 | tf_op jit(solution)/shard_map/dynamic_slice | solution.py:482
  0.8 0.7 %constant_dynamic-slice_fusion = f32[2,4]{1,0:T(2,128)S(1)} fusion(f32[2,16]{1,0:T(2,128)} %param.32, s32[]{:T(128)S(6)} %select_n.9), kind=kLoop, calls=%fused_computation.12 | loop fusion | bytes 68 | tf_op jit(solution)/shard_map/dynamic_slice | solution.py:481
  1.6 0.1 broadcast_in_dim.3
  1.6 0.1 reshape_reshape.3.skip
  1.7 0.7 %copy.26 = bf16[1,3,2,128]{3,1,2,0:T(4,128)(2,1)S(1)} copy(bf16[1,3,2,128]{3,2,1,0:T(2,128)(2,1)} %bitcast.23) | data formatting | bytes 3072
  2.4 0.1 reshape.33.rate
  2.5 0.7 %maximum_convert_fusion.taps = f32[3,512]{1,0:T(4,128)S(1)} fusion(bf16[3,256]{1,0:T(4,128)(2,1)S(1)} %bitcast.22, bf16[3,256]{1,0:T(4,128)(2,1)} %param.30), kind=kLoop, calls=%fused_computation.3 | loop fusion | flops 6144 | bytes 9216 | tf_op jit(solution)/shard_map/convert_element_type | solution.py:483
  3.2 0.0 copy-done
  3.2 1.2 %fusion.1 = f32[2,3,512]{2,0,1:T(2,128)S(1)} fusion(bf16[256,3,512]{2,0,1:T(8,128)(2,1)S(1)} %copy-done, s32[]{:T(128)S(6)} %select_n.8, f32[1,2048]{1,0:T(1,128)} %bitcast.20, f32[1,2048]{1,0:T(1,128)} %bitcast.21), kind=kOutput, calls=%fused_computation.7 | convolution fusion | flops 9439744 | bytes 815108 | tf_op jit(solution)/shard_map/sd,dkc->skc/dot_general | solution.py:474
  4.4 0.9 %dynamic-slice_bitcast_fusion = bf16[2,4,2048]{2,1,0:T(4,128)(2,1)S(1)} fusion(bf16[2048,2,16]{0,2,1:T(8,128)(2,1)} %param.29, s32[]{:T(128)S(6)} %select_n.9), kind=kLoop, calls=%fused_computation | loop fusion | bytes 65540 | tf_op jit(solution)/shard_map/transpose | solution.py:479
  5.3 0.0 copy-start.1
  5.3 1.2 %copy-done.1 = bf16[2048,256]{1,0:T(8,128)(2,1)S(1)} copy-done((bf16[2048,256]{1,0:T(8,128)(2,1)S(1)}, bf16[2048,256]{1,0:T(8,128)(2,1)}, u32[]{:S(2)}) %copy-start.1) | copy-done | bytes 1048600
  6.5 1.2 %copy-done.2 = bf16[2048,256]{1,0:T(8,128)(2,1)S(1)} copy-done((bf16[2048,256]{1,0:T(8,128)(2,1)S(1)}, bf16[2048,256]{1,0:T(8,128)(2,1)}, u32[]{:S(2)}) %copy-start.2) | copy-done | bytes 1048600
  7.7 1.2 %copy-done.3 = bf16[256,2048]{1,0:T(8,128)(2,1)S(1)} copy-done((bf16[256,2048]{1,0:T(8,128)(2,1)S(1)}, bf16[256,2048]{1,0:T(8,128)(2,1)}, u32[]{:S(2)}) %copy-start.3) | copy-done | bytes 1048600
  9.0 1.0 %copy-done.4 = bf16[2048,128]{1,0:T(8,128)(2,1)S(1)} copy-done((bf16[2048,128]{1,0:T(8,128)(2,1)S(1)}, bf16[2048,128]{1,0:T(8,128)(2,1)}, u32[]{:S(2)}) %copy-start.4) | copy-done | bytes 524312
  10.0 1.0 %copy-done.5 = bf16[2048,128]{1,0:T(8,128)(2,1)S(1)} copy-done((bf16[2048,128]{1,0:T(8,128)(2,1)S(1)}, bf16[2048,128]{1,0:T(8,128)(2,1)}, u32[]{:S(2)}) %copy-start.5) | copy-done | bytes 524312
  11.0 0.9 %copy-done.6 = bf16[32,2048]{1,0:T(8,128)(2,1)S(1)} copy-done((bf16[32,2048]{1,0:T(8,128)(2,1)S(1)}, bf16[32,2048]{1,0:T(8,128)(2,1)}, u32[]{:S(2)}) %copy-start.6) | copy-done | bytes 131096
  11.9 0.7 %copy-done.7 = f32[2048]{0:T(1024)S(1)} copy-done((f32[2048]{0:T(1024)S(1)}, f32[2048]{0:T(1024)}, u32[]{:S(2)}) %copy-start.7) | copy-done | bytes 8216
  12.6 0.7 %copy-done.8 = f32[2048]{0:T(1024)S(1)} copy-done((f32[2048]{0:T(1024)S(1)}, f32[2048]{0:T(1024)}, u32[]{:S(2)}) %copy-start.8) | copy-done | bytes 8216
  13.3 0.7 %copy-done.9 = f32[2,4,128]{2,1,0:T(4,128)S(1)} copy-done((f32[2,4,128]{2,1,0:T(4,128)S(1)}, f32[2,4,128]{2,1,0:T(4,128)}, u32[]{:S(2)}) %copy-start.9) | copy-done | bytes 4120
  14.0 0.7 %copy-done.10 = f32[256]{0:T(256)S(1)} copy-done((f32[256]{0:T(256)S(1)}, f32[256]{0:T(256)}, u32[]{:S(2)}) %copy-start.10) | copy-done | bytes 1048
  14.7 34.5 %shard_map.181 = bf16[32,2048]{1,0:T(8,128)(2,1)S(1)} custom-call(f32[8,512]{1,0:T(8,128)S(1)} %pad.8.part, bf16[32,2048]{1,0:T(8,128)(2,1)S(1)} %copy-done.6, bf16[512,2048]{1,0:T(8,128)(2,1)} %context_hbm.1, f32[1,2048]{1,0:T(1,128)S(1)} %bitcast.16, f32[1,2048]{1,0:T(1,128)S(1)} %bitcast.17, bf16[2048,256]{1,0:T(8,128)(2,1)S(1)} %copy-done.1, ...), custom_call_target="tpu_custom_call" | custom-call | tf_op jit(solution)/shard_map/pallas_call | solution.py:492
  49.2 0.7 %copy.28 = bf16[32,2048]{1,0:T(8,128)(2,1)} copy(bf16[32,2048]{1,0:T(8,128)(2,1)S(1)} %shard_map.181) | data formatting | bytes 262144
  (14 shorter events, 0.1 us)
Async XLA Ops:
  0.0 3.2 %copy-start = (bf16[256,3,512]{2,0,1:T(8,128)(2,1)S(1)}, bf16[256,3,512]{2,0,1:T(8,128)(2,1)}, u32[]{:S(2)}) copy-start(bf16[256,3,512]{2,0,1:T(8,128)(2,1)} %param.23) | copy-start | bytes 2359300
  5.3 1.2 %copy-start.1 = (bf16[2048,256]{1,0:T(8,128)(2,1)S(1)}, bf16[2048,256]{1,0:T(8,128)(2,1)}, u32[]{:S(2)}) copy-start(bf16[2048,256]{1,0:T(8,128)(2,1)} %gate_hbm.1) | copy-start | bytes 3145732
  6.5 1.2 %copy-start.2 = (bf16[2048,256]{1,0:T(8,128)(2,1)S(1)}, bf16[2048,256]{1,0:T(8,128)(2,1)}, u32[]{:S(2)}) copy-start(bf16[2048,256]{1,0:T(8,128)(2,1)} %value_hbm.1) | copy-start | bytes 3145732
  7.7 1.2 %copy-start.3 = (bf16[256,2048]{1,0:T(8,128)(2,1)S(1)}, bf16[256,2048]{1,0:T(8,128)(2,1)}, u32[]{:S(2)}) copy-start(bf16[256,2048]{1,0:T(8,128)(2,1)} %output_hbm.1) | copy-start | bytes 3145732
  8.9 1.0 %copy-start.4 = (bf16[2048,128]{1,0:T(8,128)(2,1)S(1)}, bf16[2048,128]{1,0:T(8,128)(2,1)}, u32[]{:S(2)}) copy-start(bf16[2048,128]{1,0:T(8,128)(2,1)} %write_hbm.1) | copy-start | bytes 1572868
  10.0 1.0 %copy-start.5 = (bf16[2048,128]{1,0:T(8,128)(2,1)S(1)}, bf16[2048,128]{1,0:T(8,128)(2,1)}, u32[]{:S(2)}) copy-start(bf16[2048,128]{1,0:T(8,128)(2,1)} %read_hbm.1) | copy-start | bytes 1572868
  11.0 0.9 %copy-start.6 = (bf16[32,2048]{1,0:T(8,128)(2,1)S(1)}, bf16[32,2048]{1,0:T(8,128)(2,1)}, u32[]{:S(2)}) copy-start(bf16[32,2048]{1,0:T(8,128)(2,1)} %latent.1) | copy-start | bytes 393220
  11.9 0.7 %copy-start.7 = (f32[2048]{0:T(1024)S(1)}, f32[2048]{0:T(1024)}, u32[]{:S(2)}) copy-start(f32[2048]{0:T(1024)} %param.24) | copy-start | bytes 24580
  12.6 0.7 %copy-start.8 = (f32[2048]{0:T(1024)S(1)}, f32[2048]{0:T(1024)}, u32[]{:S(2)}) copy-start(f32[2048]{0:T(1024)} %param.37) | copy-start | bytes 24580
  13.3 0.7 %copy-start.9 = (f32[2,4,128]{2,1,0:T(4,128)S(1)}, f32[2,4,128]{2,1,0:T(4,128)}, u32[]{:S(2)}) copy-start(f32[2,4,128]{2,1,0:T(4,128)} %param.33) | copy-start | bytes 12292
  14.0 0.7 %copy-start.10 = (f32[256]{0:T(256)S(1)}, f32[256]{0:T(256)}, u32[]{:S(2)}) copy-start(f32[256]{0:T(256)} %param.35) | copy-start | bytes 3076

commit v2 on v1

--- a/solution.py
+++ b/solution.py
@@ -75,20 +75,23 @@
 
 
 def kernel(
-    part, latent, context_hbm, norm_gain, post_gain, gate_hbm, value_hbm, write_hbm, read_hbm,
-    step, taps, rate, jump, skip, group_gain, output_hbm,
+    latent_hbm, context_hbm, cond_hbm, ccond_hbm, mod_hbm, norm_hbm, gate_hbm, value_hbm,
+    write_hbm, read_hbm, step_hbm, vtaps_hbm, mtaps_hbm, rate_hbm, jump_hbm, skip_hbm,
+    ggain_hbm, output_hbm, post_hbm,
     out,
     context, gate_w, value_w, write_w, read_w, output_w,
+    cond, ccond, mod_w, norm_gain, step, vtaps, mtaps, rate_v, jump, skip_v, group_gain, post_gain,
+    part, picked,
     xbuf, xstat, cstat, hbuf, chid, ubuf, ucbuf, cstep,
     part_a, modbuf, stbuf, strecv, obuf, rbuf, state_c,
     load_sem, own_sem, xs_sem, xr_sem, hs_sem, hr_sem, as_sem, ar_sem, bs_sem, br_sem,
     ss_sem, sr_sem, os_sem, or_sem,
-    *, n_sp, n_tp,
+    *, n_sp, n_tp, sliced,
 ):
     sp, tp = lax.axis_index("sp"), lax.axis_index("tp")
-    rows = latent.shape[0]
+    rows = latent_hbm.shape[0]
     tokens = n_tp * rows
-    width = latent.shape[1]
+    width = latent_hbm.shape[1]
     vwidth = value_w.shape[1]
     mwidth = write_w.shape[1]
     groups = mwidth // STATE
@@ -103,14 +106,17 @@
         pltpu.make_async_copy(s, d, load_sem.at[i])
         for i, (s, d) in enumerate(
             (
-                (context_hbm, context), (value_hbm, value_w), (write_hbm, write_w),
-                (read_hbm, read_w), (gate_hbm, gate_w), (output_hbm, output_w),
+                (mod_hbm, mod_w), (cond_hbm, cond), (ccond_hbm, ccond), (context_hbm, context),
+                (norm_hbm, norm_gain), (value_hbm, value_w), (write_hbm, write_w),
+                (read_hbm, read_w), (step_hbm, step), (vtaps_hbm, vtaps), (mtaps_hbm, mtaps),
+                (rate_hbm, rate_v), (jump_hbm, jump), (skip_hbm, skip_v), (gate_hbm, gate_w),
+                (output_hbm, output_w), (ggain_hbm, group_gain), (post_hbm, post_gain),
             )
         )
     ]
-    own_x = pltpu.make_async_copy(
-        latent, xbuf.at[pl.ds(pl.multiple_of(EDGE + tp * rows, 16), rows)], own_sem
-    )
+    mine = pl.ds(pl.multiple_of(EDGE + tp * rows, 16), rows)
+    latent = xbuf.at[mine]
+    own_x = pltpu.make_async_copy(latent_hbm, latent, own_sem)
     own_x.start()
     for c in loads:
         c.start()
@@ -130,6 +136,42 @@
             src_ref=src, dst_ref=dst, send_sem=s, recv_sem=r, device_id=where, device_id_type=MESH
         )
 
+    own_x.wait()
+
+    def x_rows(t):
+        return xbuf.at[pl.ds(pl.multiple_of(EDGE + t * rows, 16), rows)]
+
+    def send_x(r):
+        return remote(latent, x_rows(tp), xs_sem.at[r], xr_sem.at[tp], tp=lax.rem(tp + r, n_tp))
+
+    def recv_x(r):
+        peer = lax.rem(tp + r, n_tp)
+        return remote(latent, x_rows(peer), xs_sem.at[r], xr_sem.at[peer], tp=peer)
+
+    for r in range(1, n_tp):
+        send_x(r).start()
+
+    for c in loads[0:3]:
+        c.wait()
+    depth = mod_w.shape[1]
+    if sliced:
+        own = pl.ds(0, depth)
+    else:
+        own = pl.ds(pl.multiple_of(sp * depth, 128), depth)
+    left_over = [silu(cond[:, own]), silu(ccond[:, own])]
+    split = []
+    for _ in range(3):
+        for v in range(2):
+            high = left_over[v].astype(BF16).astype(F32)
+            split.append(high)
+            left_over[v] = left_over[v] - high
+    split.append(jnp.zeros((10, depth), F32))
+    split = jnp.concatenate(split, axis=0).astype(BF16)
+    prods = [dotf(split, mod_w[k]) for k in range(3)]
+    lines = [p[v : v + 1] + p[v + 2 : v + 3] + p[v + 4 : v + 5] for v in range(2) for p in prods]
+    lines.append(jnp.zeros((2, part.shape[1]), F32))
+    part[...] = jnp.concatenate(lines, axis=0)
+
     def send_a(r):
         peer = lax.rem(sp + r, n_sp)
         return remote(part, part_a.at[sp], as_sem.at[r], ar_sem.at[sp], sp=peer)
@@ -142,20 +184,7 @@
     def _(r):
         send_a(r).start()
 
-    def x_rows(t):
-        return xbuf.at[pl.ds(pl.multiple_of(EDGE + t * rows, 16), rows)]
-
-    def send_x(r):
-        return remote(latent, x_rows(tp), xs_sem.at[r], xr_sem.at[tp], tp=lax.rem(tp + r, n_tp))
-
-    def recv_x(r):
-        peer = lax.rem(tp + r, n_tp)
-        return remote(latent, x_rows(peer), xs_sem.at[r], xr_sem.at[peer], tp=peer)
-
-    for r in range(1, n_tp):
-        send_x(r).start()
-
-    loads[0].wait()
+    loads[3].wait()
     stats_pass(context, cstat, ctx)
 
     total_mod = part[...]
@@ -177,7 +206,6 @@
     for r in range(1, n_tp):
         send_b(r).start()
 
-    own_x.wait()
     for r in range(1, n_tp):
         recv_x(r).wait_recv()
 
@@ -220,6 +248,7 @@
 
     for r in range(1, n_tp):
         recv_b(r).wait_recv()
+    loads[4].wait()
     mod = jnp.concatenate([modbuf[t] for t in range(n_tp)], axis=1)
     gain_l = norm_gain[...] * (1.0 + mod[1:2])
     shift_l = mod[0:1]
@@ -228,7 +257,7 @@
 
     norm_pass(xbuf, xstat, hbuf, 0, 0, tokens + 2 * EDGE, gain_l, shift_l)
 
-    for c in loads[1:5]:
+    for c in loads[5:14]:
         c.wait()
     hidden = hbuf[...]
     span = tokens + 2 * EDGE
@@ -245,23 +274,44 @@
     ubuf[:, vwidth + mwidth :] = jnp.where(inside, rounded(dotf(hidden, read_w[...])), 0.0)
     main = hbuf[EDGE : EDGE + tokens, :]
 
-    def conv(ref, at, count, lo, hi, tap_lo):
-        t = taps[:, tap_lo : tap_lo + hi - lo]
+    def conv(ref, at, count, lo, hi, t):
         return silu(
-            t[0:1] * ref[pl.ds(at - 1, count), lo:hi]
-            + t[1:2] * ref[pl.ds(at, count), lo:hi]
-            + t[2:3] * ref[pl.ds(at + 1, count), lo:hi]
-        )
-
+            t[0] * ref[pl.ds(at - 1, count), lo:hi]
+            + t[1] * ref[pl.ds(at, count), lo:hi]
+            + t[2] * ref[pl.ds(at + 1, count), lo:hi]
+        )
+
+    value_t = [vtaps[i : i + 1, :].astype(F32) for i in range(3)]
+    write_t3, read_t3 = ([mtaps[i, k : k + 1, :].astype(F32) for i in range(3)] for k in range(2))
     nrow = 2 * heads
-    values = conv(ubuf, EDGE, tokens, 0, vwidth, 0)
-    writes = conv(ubuf, EDGE, tokens, vwidth, vwidth + mwidth, vwidth)
-    reads = conv(ubuf, EDGE, tokens, vwidth + mwidth, vwidth + 2 * mwidth, vwidth + mwidth)
+    values = conv(ubuf, EDGE, tokens, 0, vwidth, value_t)
+    writes = conv(ubuf, EDGE, tokens, vwidth, vwidth + mwidth, write_t3)
+    reads = conv(ubuf, EDGE, tokens, vwidth + mwidth, vwidth + 2 * mwidth, read_t3)
     writes_b = writes.astype(BF16)
     reads_b = reads.astype(BF16)
 
-    size = softplus(rounded(dot_nt(step[...], main)))[:nrow]
-    decay = -size * rate[...] + jump[...]
+    every = step.shape[0] // 2
+    head_at = tp * heads
+
+    def own_steps(hid):
+        picked[...] = dot_nt(step[...], hid)
+        rows_d = [picked[pl.ds(d * every + head_at, heads), :] for d in range(2)]
+        return softplus(rounded(jnp.concatenate(rows_d, axis=0)))
+
+    at_row = lax.broadcasted_iota(jnp.int32, (nrow, every), 0)
+    at_lane = lax.broadcasted_iota(jnp.int32, (nrow, every), 1)
+    rates = jnp.where(at_row < heads, rate_v[0:1, :], rate_v[1:2, :])
+    rate = jnp.sum(
+        jnp.where(at_lane == head_at + lax.rem(at_row, heads), rates, 0.0), axis=1, keepdims=True
+    )
+    head_of = lax.broadcasted_iota(jnp.int32, (1, vwidth), 1) // HEAD_DIM
+    line = lax.broadcasted_iota(jnp.int32, (1, every), 1)
+    skip = jnp.zeros((1, vwidth), F32)
+    for h in range(heads):
+        own_skip = jnp.sum(jnp.where(line == head_at + h, skip_v[...], 0.0), axis=1, keepdims=True)
+        skip = jnp.where(head_of == h, own_skip, skip)
+    size = own_steps(main)
+    decay = -size * rate + jump[...]
     forward = lax.broadcasted_iota(jnp.int32, (nrow, 1), 0) < heads
     upto = tri_of(CHUNK, lambda k, i: k <= i)
     since = tri_of(CHUNK, lambda k, i: k >= i)
@@ -322,10 +372,10 @@
         hid = chid[...]
         ucbuf[8 + i * CHUNK : 8 + (i + 1) * CHUNK, 0:vwidth] = rounded(dotf(hid, value_w[...]))
         ucbuf[8 + i * CHUNK : 8 + (i + 1) * CHUNK, vwidth:] = rounded(dotf(hid, write_w[...]))
-        cstep[i] = softplus(rounded(dot_nt(step[...], hid)))[:nrow]
+        cstep[i] = own_steps(hid)
 
     n_chunk = ctx // CHUNK
-    decays = [-cstep[i] * rate[...] for i in range(n_chunk)]
+    decays = [-cstep[i] * rate for i in range(n_chunk)]
     totals = [jnp.sum(a, axis=1, keepdims=True) for a in decays]
     entering = [None, None]
     for i in range(n_chunk):
@@ -336,8 +386,8 @@
             forward, dot32(decays[i], after) + later, dot32(decays[i], before) + earlier
         )
         ccols = columns_of(cstep[i] * jnp.exp(rest_c))
-        cvals = conv(ucbuf, 8 + i * CHUNK, CHUNK, 0, vwidth, 0)
-        cwrite_t = conv(ucbuf, 8 + i * CHUNK, CHUNK, vwidth, vwidth + mwidth, vwidth).T.astype(BF16)
+        cvals = conv(ucbuf, 8 + i * CHUNK, CHUNK, 0, vwidth, value_t)
+        cwrite_t = conv(ucbuf, 8 + i * CHUNK, CHUNK, vwidth, vwidth + mwidth, write_t3).T.astype(BF16)
         for d in range(2):
             st = states(cwrite_t, cvals, lambda r: ccols[:, r : r + 1], d)
             entering[d] = st if entering[d] is None else entering[d] + st
@@ -360,9 +410,10 @@
                 mix = mix + jnp.where(keep, jnp.exp(gap) * size[r : r + 1, :], 0.0)
             made.append(dotf((score * mix).astype(BF16), vg))
         inner.append(by_head(lambda h: made[h - g * per], g))
-    mixer = skip[...] * values + jnp.concatenate(inner, axis=1)
-
-    loads[5].wait()
+    mixer = skip * values + jnp.concatenate(inner, axis=1)
+
+    for c in loads[14:]:
+        c.wait()
     gate = silu(rounded(dotf(main, gate_w[...])))
 
     def join(k, state):
@@ -469,19 +520,12 @@
     tokens = rows * n_tp
     own_rows = modulation_weight.shape[0]
     share = modulation_weight.shape[2]
-    conditions = jax.nn.silu(jnp.stack([condition, context_condition]))
-    own = lax.dynamic_slice_in_dim(conditions, sp * own_rows, own_rows, 1)
-    part = jnp.einsum("sd,dkc->skc", own, modulation_weight.astype(F32), precision=HIGHEST)
-    part = jnp.pad(part.reshape(6, share), ((0, 2), (0, 0)))
-    head_at = tp * heads
     nrow = 2 * heads
-    step = lax.dynamic_slice_in_dim(step_weight, head_at, heads, 2)
-    step = step.transpose(1, 2, 0).reshape(nrow, width)
-    step = jnp.pad(step, ((0, -nrow % 16), (0, 0)))
-    rate = lax.dynamic_slice_in_dim(decay_rate, head_at, heads, 1).reshape(nrow, 1)
-    skip = jnp.repeat(lax.dynamic_slice_in_dim(skip_gain, head_at, heads, 0), HEAD_DIM).reshape(1, vwidth)
-    taps = jnp.concatenate([value_taps, map_taps.reshape(3, -1)], axis=1).astype(F32)
-    jump = decay_jump.reshape(nrow, tokens)
+    conds = [condition.reshape(1, -1), context_condition.reshape(1, -1)]
+    sliced = own_rows % 128 != 0
+    if sliced:
+        conds = [lax.dynamic_slice_in_dim(c, sp * own_rows, own_rows, 1) for c in conds]
+    every = decay_rate.shape[1]
     chunks = 4
     cwidth = width // chunks
     srow = mwidth + 16
@@ -490,16 +534,18 @@
     in_vmem = pl.BlockSpec(memory_space=pltpu.VMEM)
     in_any = pl.BlockSpec(memory_space=pl.ANY)
     return pl.pallas_call(
-        functools.partial(kernel, n_sp=n_sp, n_tp=n_tp),
+        functools.partial(kernel, n_sp=n_sp, n_tp=n_tp, sliced=sliced),
         out_shape=jax.ShapeDtypeStruct((rows, width), BF16),
-        in_specs=[
-            in_vmem, in_vmem, in_any, in_vmem, in_vmem, in_any, in_any, in_any, in_any,
-            in_vmem, in_vmem, in_vmem, in_vmem, in_vmem, in_vmem, in_any,
-        ],
+        in_specs=[in_any] * 19,
         out_specs=in_vmem,
         scratch_shapes=[
             vm((ctx, width), BF16), vm((width, vwidth), BF16), vm((width, vwidth), BF16),
             vm((width, mwidth), BF16), vm((width, mwidth), BF16), vm((vwidth, width), BF16),
+            vm(conds[0].shape, F32), vm(conds[0].shape, F32), vm((3, own_rows, share), BF16),
+            vm((1, width), F32), vm((2 * every, width), BF16), vm((3, vwidth), BF16),
+            vm((3, 2, mwidth), BF16), vm((2, every), F32), vm((nrow, tokens), F32),
+            vm((1, every), F32), vm((1, vwidth), F32), vm((1, width), F32),
+            vm((8, share), F32), vm((2 * every, CHUNK), F32),
             vm((tokens + 2 * EDGE, width), BF16), vm((tokens + 2 * EDGE, 128), F32),
             vm((ctx, 128), F32), vm((tokens + 2 * EDGE, width), BF16), vm((CHUNK, width), BF16),
             vm((tokens + 2 * EDGE, vwidth + 2 * mwidth), F32), vm((ctx + 16, vwidth + mwidth), F32),
@@ -508,17 +554,19 @@
             vm((2, srow, gwidth), BF16), vm((n_sp, srow, gwidth), BF16),
             vm((chunks, n_tp, rows, cwidth), BF16), vm((chunks, n_tp, rows, cwidth), BF16),
             vm((2, mwidth, gwidth), F32),
-            dma((6,)), dma, dma((n_tp,)), dma((n_tp,)), dma((2,)), dma((2,)),
+            dma((18,)), dma, dma((n_tp,)), dma((n_tp,)), dma((2,)), dma((2,)),
             dma((n_sp,)), dma((n_sp,)), dma((n_tp,)), dma((n_tp,)), dma((n_sp,)), dma((n_sp,)),
             dma((chunks, n_tp)), dma((chunks, n_tp)),
         ],
         compiler_params=pltpu.CompilerParams(
-            collective_id=0, has_side_effects=True, vmem_limit_bytes=48 * 1024 * 1024
+            collective_id=0, has_side_effects=True, vmem_limit_bytes=62 * 1024 * 1024
         ),
     )(
-        part, latent, context, norm_gain.reshape(1, -1), post_gain.reshape(1, -1), gate_weight,
-        value_weight, write_weight, read_weight, step, taps, rate, jump, skip,
-        group_gain.reshape(1, -1), output_weight,
+        latent, context, *conds, modulation_weight.transpose(1, 0, 2), norm_gain.reshape(1, -1),
+        gate_weight, value_weight, write_weight, read_weight,
+        step_weight.transpose(1, 2, 0).reshape(2 * every, width), value_taps, map_taps, decay_rate,
+        decay_jump.reshape(nrow, tokens), skip_gain.reshape(1, -1), group_gain.reshape(1, -1),
+        output_weight, post_gain.reshape(1, -1),
     )
 
 

time: 50.5 us -> 37.6 us (0.74)
  local copies, waits for them, and re-layouts: 13.4 us -> 1.57 us
  matrix products: 1.17 us -> 0 us
  Pallas kernels: 34.5 us -> 35.6 us
  other arithmetic: 0.69 us -> 0 us
    unnamed x24 -> x1, local copies, waits for them, and re-layouts: 10.8 us -> 1.57 us
    dynamic_slice x2 -> x0, local copies, waits for them, and re-layouts: 1.55 us -> none  [the longest x1 0.8 us: body(): lax.dynamic_slice_in_dim(skip_gain, head_at, heads, 0)]
    dot_general x1 -> x0, matrix products: 1.17 us -> none  [body(): jnp.einsum('sd,dkc->skc', own, modulation_weight.astype(F32), precision=H...]
    pallas_call x1, Pallas kernels: 34.5 us -> 35.6 us  [body(): pl.pallas_call(functools.partial(kernel, n_sp=n_sp, n_tp=n_tp, sliced=sli...]
    transpose x1 -> x0, local copies, waits for them, and re-layouts: 0.87 us -> none  [body(): step = step.transpose(1, 2, 0).reshape(nrow, width)]
    convert_element_type x1 -> x0, other arithmetic: 0.69 us -> none  [body(): jnp.concatenate([value_taps, map_taps.reshape(3, -1)], axis=1).astype(F32)]
where the time goes in v2:
time: 37.6 us; the launch traced here: 37.2 us
  Pallas kernels  35.6 us (95%)
  local copies, waits for them, and re-layouts  1.57 us (4%)
    pallas_call x1, Pallas kernels, body(): pl.pallas_call(functools.partial(kernel, n_sp=n_sp, n_tp=n_tp, sliced=sli...  35.6 us
    unnamed x1, local copies, waits for them, and re-layouts  1.57 us

profile of v2, /device:TPU:0, one launch (start us, length us, event | category | flops | bytes accessed | tf_op | source)
XLA Modules:
  0.0 37.2 jit_solution(14603240750386581589)
XLA Ops:
  0.0 35.6 %shard_map.181 = bf16[32,2048]{1,0:T(8,128)(2,1)} custom-call(bf16[32,2048]{1,0:T(8,128)(2,1)} %latent_hbm.1, bf16[512,2048]{1,0:T(8,128)(2,1)} %context_hbm.1, f32[1,2048]{1,0:T(1,128)} %bitcast.13, f32[1,2048]{1,0:T(1,128)} %bitcast.14, bf16[3,256,512]{2,1,0:T(8,128)(2,1)} %bitcast.11, f32[1,2048]{1,0:T(1,128)} %bitcast.15, bf16[2048,256]{1,0:T(8,128)(2,1)} %gate_hbm.1, ...), custom_call_target="tpu_custom_call" | custom-call | tf_op jit(solution)/shard_map/pallas_call | solution.py:536
  35.6 1.6 %copy.21 = bf16[32,2048]{1,0:T(8,128)(2,1)} copy(bf16[32,2048]{1,0:T(8,128)(2,1)} %shard_map.181) | data formatting | bytes 262144
